TPU v7x, 32 devices: a whole 2x2x4 slice. The times are simulated.
32 devices in a mesh: kv: 8 (over z, y), tp: 4 (over x, core).
Axes of the slice: x: 2, y: 2, z: 4, core: 2. Of those that a mesh axis runs over, the one named last changes fastest.
Arguments:
- tokens: bfloat16 [256, 4, 2048], P(None, None, ('kv', 'tp')), may hold values from -520 to 520
- input_norm_gain: bfloat16 [2048], replicated, may hold values from 0.099609375 to 1.8984375
- query_weight: bfloat16 [2048, 2048], P(None, 'kv'), may hold values from -0.125 to 0.125
- key_weight: bfloat16 [2048, 2048], P(None, 'kv'), may hold values from -0.125 to 0.125
- value_weight: bfloat16 [2048, 16, 128], P(None, 'kv', 'tp'), may hold values from -1.14904852 to 1.14904852
- output_gate_weight: bfloat16 [2048, 16, 128], P(None, 'kv', 'tp'), may hold values from -0.125 to 0.125
- strength_weight: bfloat16 [2048, 16], P(None, 'kv'), may hold values from -0.125 to 0.125
- decay_weight: bfloat16 [2048, 16], P(None, 'kv'), may hold values from -0.125 to 0.125
- head_decay_rate: float32 [16], P('kv'), may hold values from 0.005 to 1.5
- proposal_log_decay: float32 [256, 4, 16], P(None, None, 'kv'), may hold values from -0.69 to 0
- head_norm_gain: bfloat16 [128], P('tp'), may hold values from 0.099609375 to 1.8984375
- output_weight: bfloat16 [16, 128, 2048], P('kv', 'tp'), may hold values from -1.14904852 to 1.14904852
- output_norm_gain: bfloat16 [2048], P(('kv', 'tp')), may hold values from 0.099609375 to 1.8984375
- state: float32 [256, 16, 128, 128], P(None, 'kv', 'tp'), may hold values from -4.5961941 to 4.5961941
- previous_keys: bfloat16 [256, 4, 2048], P(None, None, 'kv'), may hold values from -6 to 6
- previous_values: bfloat16 [256, 4, 16, 128], P(None, None, 'kv', 'tp'), may hold values from -52 to 52
- previous_log_decay: float32 [256, 4, 16], P(None, None, 'kv'), may hold values from -0.7 to -0.02
- previous_strengths: float32 [256, 4, 16], P(None, None, 'kv'), may hold values from 0.1 to 0.9
- accepted: int32 [256], replicated, may hold values from 0 to 4
- parent: int32 [256, 4], replicated, may hold values from -1 to 2, as said below
Outputs:
- layer_out: bfloat16 [256, 4, 2048], P(None, None, ('kv', 'tp'))
- accepted_state: float32 [256, 16, 128, 128], P(None, 'kv', 'tp')
Inputs may be any that keep to these rules, and one draw needn't show every extreme that they name: parent[b, i] is -1 or a proposal index below i; -1 means that proposal i follows the accepted old proposals directly.
All inputs are finite; a program needn't handle non-finite values.
Results may differ from a plain program's by a relative error of at most 0.019.
Values may be sent and summed in bfloat16 or wider, within the bound.
A program may use at most 128 MiB of HBM per device.

v0:
```python
import jax
import jax.numpy as jnp
from jax import lax
from jax.sharding import PartitionSpec as P

epsilon = 1e-06


def unit_rows(matrix):
    return matrix * lax.rsqrt(jnp.sum(matrix * matrix, axis=-1, keepdims=True) + epsilon)


def exact_product(form, left, right):
    return jnp.einsum(form, left, right, precision=lax.Precision.HIGHEST)


def visibility(parent):
    sequence_count, proposal_count = parent.shape
    position = jnp.arange(proposal_count, dtype=jnp.int32)
    parent_hot = (parent[:, :, None] == position[None, None, :]).astype(jnp.float32)
    ancestry = []
    for row_index in range(proposal_count):
        ancestor_row = parent_hot[:, row_index, :]
        if row_index > 0:
            earlier = jnp.stack(ancestry, axis=1)
            ancestor_row = ancestor_row + exact_product(
                "bj,bjk->bk", parent_hot[:, row_index, :row_index], earlier
            )
        ancestry.append(ancestor_row)
    ancestor = jnp.stack(ancestry, axis=1)
    chain = (position[:, None] > position[None, :]).astype(jnp.float32)
    upper = jnp.concatenate(
        [
            jnp.broadcast_to(chain, (sequence_count, proposal_count, proposal_count)),
            jnp.zeros((sequence_count, proposal_count, proposal_count), jnp.float32),
        ],
        axis=2,
    )
    lower = jnp.concatenate(
        [jnp.ones((sequence_count, proposal_count, proposal_count), jnp.float32), ancestor], axis=2
    )
    return jnp.concatenate([upper, lower], axis=1)


def split_heads(matrix, sequence_count, proposal_count, number_of_heads):
    return (
        matrix.astype(jnp.float32)
        .reshape(sequence_count, proposal_count, number_of_heads, -1)
        .transpose(0, 2, 1, 3)
    )


def delta_recursion(
    query_projected,
    key_projected,
    value_projected,
    output_gate_logits,
    write_strength_logits,
    decay_logits,
    decay_speed,
    proposal_group,
    head_norm_gain,
    state,
    previous_keys,
    previous_values,
    previous_log_decay,
    previous_strengths,
    accepted,
    parent,
    channel_count_total,
):
    sequence_count, number_of_heads, value_dim, head_dim = state.shape
    proposal_count = parent.shape[1]
    queries = unit_rows(
        split_heads(query_projected, sequence_count, proposal_count, number_of_heads)
    ) * head_dim ** (-0.5)
    new_keys = unit_rows(
        split_heads(key_projected, sequence_count, proposal_count, number_of_heads)
    )
    old_keys = unit_rows(
        split_heads(previous_keys, sequence_count, proposal_count, number_of_heads)
    )
    new_values = split_heads(value_projected, sequence_count, proposal_count, number_of_heads)
    old_values = split_heads(previous_values, sequence_count, proposal_count, number_of_heads)
    zgate = split_heads(output_gate_logits, sequence_count, proposal_count, number_of_heads)
    beta_new = jax.nn.sigmoid(
        write_strength_logits.reshape(sequence_count, proposal_count, number_of_heads)
    ).transpose(0, 2, 1)
    fresh_decay = (
        -decay_speed[None, None, :]
        * jax.nn.softplus(decay_logits.reshape(sequence_count, proposal_count, number_of_heads))
        + proposal_group
    ).transpose(0, 2, 1)
    position = jnp.arange(proposal_count, dtype=jnp.int32)
    live = (position[None, :] < accepted[:, None]).astype(jnp.float32)[:, None, :]
    beta_old = previous_strengths.transpose(0, 2, 1) * live
    decay_old = previous_log_decay.transpose(0, 2, 1) * live
    keys_all = jnp.concatenate([old_keys, new_keys], axis=2)
    values_all = jnp.concatenate([old_values, new_values], axis=2)
    beta_all = jnp.concatenate([beta_old, beta_new], axis=2)
    decay_all = jnp.concatenate([decay_old, fresh_decay], axis=2)
    visible = visibility(parent)
    gamma_sum = decay_all + exact_product("bij,bhj->bhi", visible, decay_all)
    gamma_diff = gamma_sum[:, :, :, None] - gamma_sum[:, :, None, :]
    decay_pair = jnp.exp(jnp.minimum(gamma_diff, 0.0)) * visible[:, None]
    coupling = (
        beta_all[..., None] * exact_product("bhid,bhjd->bhij", keys_all, keys_all) * decay_pair
    )
    right_side = jnp.concatenate(
        [beta_all[..., None] * values_all, (beta_all * jnp.exp(gamma_sum))[..., None] * keys_all],
        axis=-1,
    )
    solved = []
    for row_index in range(2 * proposal_count):
        current = right_side[:, :, row_index]
        if row_index > 0:
            current = current - exact_product(
                "bhj,bhjd->bhd", coupling[:, :, row_index, :row_index], jnp.stack(solved, axis=2)
            )
        solved.append(current)
    solution = jnp.stack(solved, axis=2)
    update = solution[..., :value_dim] - exact_product(
        "bhcd,bhed->bhce", solution[..., value_dim:], state
    )
    identity = jnp.eye(2 * proposal_count, dtype=jnp.float32)
    seen = visible[:, proposal_count:] + identity[proposal_count:][None]
    reach = jnp.exp(jnp.minimum(gamma_diff[:, :, proposal_count:], 0.0)) * seen[:, None]
    query_key = exact_product("bhid,bhjd->bhij", queries, keys_all) * reach
    readout = exact_product(
        "bhid,bhed->bhie", queries * jnp.exp(gamma_sum[:, :, proposal_count:])[..., None], state
    )
    readout = readout + exact_product("bhij,bhje->bhie", query_key, update)
    squares = channel_count_total(jnp.sum(readout * readout, axis=-1))
    readout = readout * lax.rsqrt(squares / head_dim + epsilon)[..., None]
    readout = readout * head_norm_gain.astype(jnp.float32) * jax.nn.silu(zgate)
    blended_rows = readout.transpose(0, 2, 1, 3).reshape(
        sequence_count * proposal_count, number_of_heads * value_dim
    )
    blended_rows = blended_rows.astype(jnp.bfloat16)
    last_gamma = gamma_sum[:, :, proposal_count - 1 : proposal_count]
    key_weighted = old_keys * jnp.exp(last_gamma - gamma_sum[:, :, :proposal_count])[..., None]
    accepted_state = jnp.exp(last_gamma)[..., None] * state + exact_product(
        "bhcd,bhce->bhed", key_weighted, update[:, :, :proposal_count]
    )
    return (blended_rows, accepted_state)


def channel_sum(squares):
    return lax.psum(squares, "tp")


def on_device(
    tokens,
    input_norm_gain,
    query_weight,
    key_weight,
    value_weight,
    output_gate_weight,
    strength_weight,
    decay_weight,
    head_decay_rate,
    proposal_log_decay,
    head_norm_gain,
    output_weight,
    output_norm_gain,
    state,
    previous_keys,
    previous_values,
    previous_log_decay,
    previous_strengths,
    accepted,
    parent,
):
    gathered = lax.all_gather(tokens, ("kv", "tp"), axis=2, tiled=True)
    sequence_count, proposal_count, width = gathered.shape
    row_total = sequence_count * proposal_count
    features = gathered.astype(jnp.float32)
    normed = features * lax.rsqrt(jnp.mean(features * features, axis=-1, keepdims=True) + epsilon)
    normed = (normed * input_norm_gain.astype(jnp.float32)).astype(jnp.bfloat16)
    flat_rows = normed.reshape(row_total, width)
    write_strength_logits = jnp.dot(flat_rows, strength_weight, preferred_element_type=jnp.float32)
    decay_logits = jnp.dot(flat_rows, decay_weight, preferred_element_type=jnp.float32)
    value_projected = jnp.dot(
        flat_rows, value_weight.reshape(width, -1), preferred_element_type=jnp.float32
    ).astype(jnp.bfloat16)
    output_gate_logits = jnp.dot(
        flat_rows, output_gate_weight.reshape(width, -1), preferred_element_type=jnp.float32
    ).astype(jnp.bfloat16)
    query_projected = jnp.dot(flat_rows, query_weight, preferred_element_type=jnp.float32).astype(
        jnp.bfloat16
    )
    key_projected = jnp.dot(flat_rows, key_weight, preferred_element_type=jnp.float32).astype(
        jnp.bfloat16
    )
    blended_rows, accepted_state = delta_recursion(
        query_projected,
        key_projected,
        value_projected,
        output_gate_logits,
        write_strength_logits,
        decay_logits,
        head_decay_rate,
        proposal_log_decay,
        head_norm_gain,
        state,
        previous_keys,
        previous_values,
        previous_log_decay,
        previous_strengths,
        accepted,
        parent,
        channel_sum,
    )
    partial_out = jnp.dot(
        blended_rows, output_weight.reshape(-1, width), preferred_element_type=jnp.float32
    )
    own_cols = output_norm_gain.shape[0]
    totals = lax.psum(partial_out, ("kv", "tp"))
    scaling = lax.rsqrt(jnp.mean(totals * totals, axis=-1, keepdims=True) + epsilon)
    own_index = lax.axis_index("kv") * lax.axis_size("tp") + lax.axis_index("tp")
    share = lax.dynamic_slice_in_dim(totals, own_index * own_cols, own_cols, 1)
    layer_out = (share * scaling * output_norm_gain.astype(jnp.float32)).astype(jnp.bfloat16)
    return (layer_out.reshape(sequence_count, proposal_count, own_cols), accepted_state)


def solution(mesh):
    placed = (
        P(None, None, ("kv", "tp")),
        P(),
        P(None, "kv"),
        P(None, "kv"),
        P(None, "kv", "tp"),
        P(None, "kv", "tp"),
        P(None, "kv"),
        P(None, "kv"),
        P("kv"),
        P(None, None, "kv"),
        P("tp"),
        P("kv", "tp", None),
        P(("kv", "tp")),
        P(None, "kv", "tp", None),
        P(None, None, "kv"),
        P(None, None, "kv", "tp"),
        P(None, None, "kv"),
        P(None, None, "kv"),
        P(),
        P(),
    )
    return jax.shard_map(
        on_device,
        mesh=mesh,
        in_specs=placed,
        out_specs=(P(None, None, ("kv", "tp")), P(None, "kv", "tp", None)),
        check_vma=False,
    )
```

profile of v0, /device:TPU:0, one launch (start us, length us, event | category | flops | bytes accessed | tf_op | source)
XLA Modules:
  0.0 489.5 jit_solution(4462959712660813374)
XLA Ops:
  11.4 2.1 fusion.18
  16.0 1.6 fusion.16
  17.7 58.3 %all-gather.2.cloned.1.call-done = bf16[256,4,2048]{0,2,1:T(8,128)(2,1)} async-done(((bf16[256,4,64]{0,2,1:T(8,128)(2,1)}), bf16[256,4,2048]{0,2,1:T(8,128)(2,1)}) %all-gather.2.cloned.1.call-update) | async-done | bytes 4194320 | tf_op jit(solution)/shard_map/all_gather | solution.py:174
  76.1 3.2 fusion
  79.5 2.7 fusion.2
  82.2 7.9 %copy.594 = bf16[256,4,2048]{2,1,0:T(4,128)(2,1)} copy(bf16[256,4,2048]{0,2,1:T(8,128)(2,1)} %fusion.2) | data formatting | bytes 8388608 | tf_op jit(solution)/shard_map/convert_element_type | solution.py:179
  90.2 3.0 fusion.61
  94.6 2.5 fusion.94
  98.4 6.9 %reshape.134 = bf16[1024,2048]{1,0:T(8,128)(2,1)} reshape(bf16[256,4,2048]{2,1,0:T(4,128)(2,1)} %copy.594) | data formatting | bytes 8388608 | tf_op jit(solution)/shard_map/reshape | solution.py:180
  105.2 3.4 fusion.9
  111.1 1.7 bitcast_multiply_fusion
  112.8 1.7 broadcast_subtract_fusion
  115.3 5.3 %multiply_multiply_fusion = f32[256,2,8,8]{3,2,1,0:T(8,128)S(1)} fusion(f32[256,2,4,128]{3,2,1,0:T(4,128)S(1)} %bitcast_multiply_fusion, f32[256,2,4,128]{3,2,1,0:T(4,128)S(1)} %fusion.16, f32[256,8,8]{2,1,0:T(8,128)S(1)} %copy-done.22, f32[256,2,8]{2,1,0:T(2,128)} %copy.621, f32[256,2,8]{2,1,0:T(2,128)S(1)} %copy.615), kind=kOutput, calls=%fused_computation.26 | convolution fusion | flops 51019776 | bytes 2326528 | tf_op jit(solution)/shard_map/bhid,bhjd->bhij/dot_general | solution.py:14
  124.4 1.4 fusion.11
  126.6 1.4 copy.663
  128.1 3.4 fusion.10
  133.5 15.6 %fusion.22 = f32[256,2,4,32]{3,2,1,0:T(4,128)S(1)} fusion(f32[256,2,32,128]{3,2,1,0:T(8,128)} %param.33, f32[256,4,2,128]{3,2,1,0:T(2,128)S(1)} %reshape.152, f32[256,2,4]{2,1,0:T(2,128)S(1)} %copy.609, f32[256,2,4]{2,1,0:T(2,128)S(1)} %copy.597), kind=kOutput, calls=%fused_computation.58 | convolution fusion | flops 101187584 | bytes 9715712 | tf_op jit(solution)/shard_map/bhid,bhed->bhie/dot_general | solution.py:14
  150.5 1.9 fusion.8
  155.5 1.7 convert_multiply_fusion.2
  157.2 10.5 %pad_maximum_fusion.7 = (f32[256,2,1,160]{3,2,1,0:T(1,128)}, f32[256,2,1,160]{3,2,1,0:T(1,128)S(1)}, f32[256,2,1,160]{3,2,1,0:T(1,128)S(1)}, f32[256,2,1,160]{3,...) fusion(f32[256,2,8,128]{3,2,1,0:T(8,128)S(1)} %fusion.8, ...), kind=kLoop, calls=%fused_computation.72 | loop fusion | flops 655360 | bytes 5242880 | tf_op jit(solution)/shard_map/concatenate | solution.py:109
  170.8 7.6 %fusion.24 = f32[256,2,1,160]{3,2,1,0:T(1,128)} fusion(f32[256,2,1,160]{3,2,1,0:T(1,128)S(1)} %copy.650, f32[256,2,1,160]{3,2,1,0:T(1,128)S(1)} %get-tuple-element.41, f32[256,2,8,8]{3,2,1,0:T(8,128)} %copy-done.6), kind=kOutput, calls=%fused_computation.60 | convolution fusion | flops 2129920 | bytes 1245184 | tf_op jit(solution)/shard_map/bhj,bhjd->bhd/dot_general | solution.py:14
  182.9 2.0 copy.633
  184.9 1.9 constant_dynamic-update-slice_fusion.7
  186.8 2.1 copy.652
  188.9 8.4 %fusion.5 = f32[256,2,1,160]{3,2,1,0:T(1,128)} fusion(f32[256,2,1,160]{3,2,1,0:T(1,128)} %copy.652, f32[256,2,1,160]{3,2,1,0:T(1,128)} %copy.651, f32[256,2,1,160]{3,2,1,0:T(1,128)} %copy-done.8, f32[256,2,1,160]{3,2,1,0:T(1,128)S(1)} %get-tuple-element.41, f32[256,2,8,8]{3,2,1,0:T(8,128)S(1)} %copy-done.7), kind=kOutput, calls=%fused_computation.28 | convolution fusion | flops 4915200 | bytes 2097152 | tf_op jit(solution)/shard_map/bhj,bhjd->bhd/dot_general | solution.py:14
  197.3 1.8 copy.686
  199.1 1.8 copy.635
  201.0 1.9 constant_dynamic-update-slice_fusion.6
  202.9 1.9 copy.653
  206.4 1.7 constant_dynamic-update-slice_fusion.1
  210.3 1.6 multiply_reduce_fusion.2
  212.9 1.9 copy.654
  216.3 1.8 multiply_reduce_fusion.1
  218.9 1.9 copy.655
  220.7 11.4 %stack.101 = f32[256,2,7,160]{3,2,1,0:T(8,128)} concatenate(f32[256,2,1,160]{3,2,1,0:T(1,128)S(1)} %get-tuple-element.41, f32[256,2,1,160]{3,2,1,0:T(1,128)S(1)} %copy-done.9, f32[256,2,1,160]{3,2,1,0:T(1,128)} %copy.651, f32[256,2,1,160]{3,2,1,0:T(1,128)} %copy.652, f32[256,2,1,160]{3,2,1,0:T(1,128)} %copy.653, f32[256,2,1,160]{3,2,1,0:T(1,128)} %copy.654, f32[256,2,1,160]{3,2,1,0:T(1,128)} %copy.655), dimensions={2} | concatenate | bytes 4587520 | tf_op jit(solution)/shard_map/stack | solution.py:118
  232.2 7.2 %fusion.48 = f32[256,2,1,160]{3,2,1,0:T(1,128)} fusion(f32[256,2,7,160]{3,2,1,0:T(8,128)} %stack.101, f32[256,2,8,8]{3,2,1,0:T(8,128)S(1)} %copy-done.7), kind=kOutput, calls=%fused_computation.96 | convolution fusion | flops 6881280 | bytes 2883584 | tf_op jit(solution)/shard_map/bhj,bhjd->bhd/dot_general | solution.py:14
  240.7 1.9 copy.643
  242.5 1.7 fusion.40
  244.3 1.9 copy.656
  246.2 11.2 %stack.103 = f32[256,2,8,160]{3,2,1,0:T(8,128)} concatenate(f32[256,2,1,160]{3,2,1,0:T(1,128)S(1)} %get-tuple-element.41, f32[256,2,1,160]{3,2,1,0:T(1,128)S(1)} %copy-done.9, f32[256,2,1,160]{3,2,1,0:T(1,128)S(1)} %copy-done.10, f32[256,2,1,160]{3,2,1,0:T(1,128)S(1)} %copy-done.11, f32[256,2,1,160]{3,2,1,0:T(1,128)S(1)} %copy-done.12, f32[256,2,1,160]{3,2,1,0:T(1,128)S(1)} %copy-done.13, ...), dimensions={2} | concatenate | bytes 5242880 | tf_op jit(solution)/shard_map/stack | solution.py:121
  257.4 16.8 %slice_subtract_fusion = f32[256,2,8,32]{3,2,1,0:T(8,128)S(1)} fusion(f32[256,2,8,160]{3,2,1,0:T(8,128)} %stack.103, f32[256,2,32,128]{3,2,1,0:T(8,128)} %param.33), kind=kOutput, calls=%fused_computation.23 | convolution fusion | flops 201457664 | bytes 11534336 | tf_op jit(solution)/shard_map/bhcd,bhed->bhce/dot_general | solution.py:14
  274.3 4.2 convolution_multiply_fusion
  278.6 3.4 fusion.95
  284.3 6.4 %psum.14 = f32[256,2,4]{0,2,1:T(4,128)S(1)} all-reduce(f32[256,2,4]{0,2,1:T(4,128)S(1)} %copy.659), channel_id=1, replica_groups=mesh['kv'=8,'tp'=4] {'tp'}, use_global_device_ids=true, to_apply=%region_5.6 | all-reduce | flops 2048 | bytes 16384 | tf_op jit(solution)/shard_map/psum | solution.py:149
  292.8 4.5 fusion.96
  298.4 18.9 %multiply_add_fusion = f32[256,2,32,128]{3,2,1,0:T(8,128)} fusion(f32[256,2,32,128]{3,2,1,0:T(8,128)} %param.33, f32[256,2]{1,0:T(8,128)S(1)} %bitcast.222, f32[256,2,8,32]{3,2,1,0:T(8,128)S(1)} %slice_subtract_fusion, f32[256,2,4]{2,1,0:T(2,128)S(1)} %copy.666, bf16[256,4,256]{2,1,0:T(4,128)(2,1)S(1)} %copy-done.26, f32[256,2,4]{2,1,0:T(2,128)S(1)} %copy-done.32), kind=kOutput, calls=%fused_computation.19 | convolution fusion | flops 105644032 | bytes 19005440 | tf_op jit(solution)/shard_map/bhcd,bhce->bhed/dot_general | solution.py:14
  317.2 158.6 %all-reduce.4.cloned.1.call-done = f32[1024,2048]{1,0:T(8,128)} async-done(((f32[1024,2048]{1,0:T(8,128)}), f32[1024,2048]{1,0:T(8,128)}) %all-reduce.4.cloned.1.call-update) | async-done | bytes 8388624 | tf_op jit(solution)/shard_map/psum | solution.py:218
  475.8 4.1 multiply_reduce_fusion
  (202 shorter events, 47.0 us)
Async XLA Ops:
  7.2 98.1 %copy-start = (bf16[2048,256]{1,0:T(8,128)(2,1)S(1)}, bf16[2048,256]{1,0:T(8,128)(2,1)}, u32[]{:S(2)}) copy-start(bf16[2048,256]{1,0:T(8,128)(2,1)} %param.23) | copy-start | bytes 3145732
  7.2 7.7 %copy-start.41 = (bf16[256,4,2,32]{0,3,2,1:T(8,128)(2,1)S(1)}, bf16[256,4,2,32]{0,3,2,1:T(8,128)(2,1)}, u32[]{:S(2)}) copy-start(bf16[256,4,2,32]{0,3,2,1:T(8,128)(2,1)} %param.35) | copy-start | bytes 393220
  7.2 8.8 %copy-start.47 = (s32[256]{0:T(256)S(1)}, s32[256]{0:T(256)}, u32[]{:S(2)}) copy-start(s32[256]{0:T(256)} %param.38) | copy-start | bytes 3076
  7.2 8.8 %copy-start.44 = (f32[256,4,2]{0,2,1:T(2,128)S(1)}, f32[256,4,2]{0,2,1:T(2,128)}, u32[]{:S(2)}) copy-start(f32[256,4,2]{0,2,1:T(2,128)} %param.36) | copy-start | bytes 24580
  7.2 8.8 %copy-start.45 = (f32[256,4,2]{0,2,1:T(2,128)S(1)}, f32[256,4,2]{0,2,1:T(2,128)}, u32[]{:S(2)}) copy-start(f32[256,4,2]{0,2,1:T(2,128)} %param.37) | copy-start | bytes 24580
  7.2 68.8 %all-gather.2.cloned.1.call-start = ((), (), s32[]{:S(2)}) async-start(), calls=%async_computation | async-start | bytes 4325376 | tf_op jit(solution)/shard_map/all_gather | solution.py:174
  8.0 467.8 %all-reduce.4.cloned.1.call-start = ((), (), s32[]{:S(2)}) async-start(), calls=%async_computation.1 | async-start | bytes 16777216 | tf_op jit(solution)/shard_map/psum | solution.py:218
  11.4 83.1 %copy-start.21 = (f32[256,8,8]{2,1,0:T(8,128)}, f32[256,8,8]{2,1,0:T(8,128)S(1)}, u32[]{:S(2)}) copy-start(f32[256,8,8]{2,1,0:T(8,128)S(1)} %copy.607) | copy-start | bytes 196612
  13.9 65.3 %copy-start.31 = (f32[256,2,4]{2,1,0:T(2,128)}, f32[256,2,4]{2,1,0:T(2,128)S(1)}, u32[]{:S(2)}) copy-start(f32[256,2,4]{2,1,0:T(2,128)S(1)} %copy.611) | copy-start | bytes 24580
  17.7 97.6 %copy-start.14 = (f32[256,2,4,128]{3,2,1,0:T(4,128)}, f32[256,2,4,128]{3,2,1,0:T(4,128)S(1)}, u32[]{:S(2)}) copy-start(f32[256,2,4,128]{3,2,1,0:T(4,128)S(1)} %fusion.16) | copy-start | bytes 3145732
  76.1 3.4 copy-start.5
  82.2 7.9 %copy-start.42 = (bf16[2048,2]{0,1:T(2,128)(2,1)S(1)}, bf16[2048,2]{0,1:T(2,128)(2,1)}, u32[]{:S(2)}) copy-start(bf16[2048,2]{0,1:T(2,128)(2,1)} %param.27) | copy-start | bytes 24580
  90.2 3.4 copy-start.2
  90.2 3.5 copy-start.43
  112.8 7.9 %copy-start.17 = (f32[256,2,4,128]{3,2,1,0:T(4,128)}, f32[256,2,4,128]{3,2,1,0:T(4,128)S(1)}, u32[]{:S(2)}) copy-start(f32[256,2,4,128]{3,2,1,0:T(4,128)S(1)} %bitcast_multiply_fusion) | copy-start | bytes 3145732
  112.8 2.5 copy-start.22
  115.3 9.1 %copy-start.3 = (bf16[1024,2048]{1,0:T(8,128)(2,1)S(1)}, bf16[1024,2048]{1,0:T(8,128)(2,1)}, u32[]{:S(2)}) copy-start(bf16[1024,2048]{1,0:T(8,128)(2,1)} %reshape.134) | copy-start | bytes 12582916
  120.7 2.8 copy-start.6
  120.7 3.7 copy-start.36
  125.8 2.3 copy-start.48
  132.1 1.4 copy-start.19
  133.5 15.6 %copy-start.39 = (f32[256,2,4]{2,1,0:T(2,128)}, f32[256,2,4]{2,1,0:T(2,128)S(1)}, u32[]{:S(2)}) copy-start(f32[256,2,4]{2,1,0:T(2,128)S(1)} %copy.597) | copy-start | bytes 24580
  149.1 1.4 copy-start.15
  150.5 2.5 copy-start.4
  150.5 2.5 copy-start.37
  157.2 11.8 %copy-start.34 = (f32[256,2,1,1]{3,2,1,0:T(1,128)S(1)}, f32[256,2,1,1]{3,2,1,0:T(1,128)}, u32[]{:S(2)}) copy-start(f32[256,2,1,1]{3,2,1,0:T(1,128)} %slice.141) | copy-start | bytes 6148
  170.8 7.6 %copy-start.8 = (f32[256,2,1,160]{3,2,1,0:T(1,128)}, f32[256,2,1,160]{3,2,1,0:T(1,128)S(1)}, u32[]{:S(2)}) copy-start(f32[256,2,1,160]{3,2,1,0:T(1,128)S(1)} %copy.650) | copy-start | bytes 983044
  170.8 8.9 %copy-start.29 = (f32[256,2,1,160]{3,2,1,0:T(1,128)S(1)}, f32[256,2,1,160]{3,2,1,0:T(1,128)}, u32[]{:S(2)}) copy-start(f32[256,2,1,160]{3,2,1,0:T(1,128)} %get-tuple-element.43) | copy-start | bytes 983044
  178.4 3.5 copy-start.33
  182.9 6.0 %copy-start.7 = (f32[256,2,8,8]{3,2,1,0:T(8,128)S(1)}, f32[256,2,8,8]{3,2,1,0:T(8,128)}, u32[]{:S(2)}) copy-start(f32[256,2,8,8]{3,2,1,0:T(8,128)} %copy-done.6) | copy-start | bytes 393220
  204.8 3.2 copy-start.23
  205.6 4.3 copy-start.28
  210.3 5.5 %copy-start.27 = (f32[256,2,1,160]{3,2,1,0:T(1,128)S(1)}, f32[256,2,1,160]{3,2,1,0:T(1,128)}, u32[]{:S(2)}) copy-start(f32[256,2,1,160]{3,2,1,0:T(1,128)} %get-tuple-element.47) | copy-start | bytes 983044
  216.3 4.5 copy-start.9
  239.3 6.8 %copy-start.10 = (f32[256,2,1,160]{3,2,1,0:T(1,128)S(1)}, f32[256,2,1,160]{3,2,1,0:T(1,128)}, u32[]{:S(2)}) copy-start(f32[256,2,1,160]{3,2,1,0:T(1,128)} %copy.651) | copy-start | bytes 983044
  239.3 6.9 %copy-start.11 = (f32[256,2,1,160]{3,2,1,0:T(1,128)S(1)}, f32[256,2,1,160]{3,2,1,0:T(1,128)}, u32[]{:S(2)}) copy-start(f32[256,2,1,160]{3,2,1,0:T(1,128)} %copy.652) | copy-start | bytes 983044
  239.3 6.9 %copy-start.12 = (f32[256,2,1,160]{3,2,1,0:T(1,128)S(1)}, f32[256,2,1,160]{3,2,1,0:T(1,128)}, u32[]{:S(2)}) copy-start(f32[256,2,1,160]{3,2,1,0:T(1,128)} %copy.653) | copy-start | bytes 983044
  239.3 6.9 %copy-start.13 = (f32[256,2,1,160]{3,2,1,0:T(1,128)S(1)}, f32[256,2,1,160]{3,2,1,0:T(1,128)}, u32[]{:S(2)}) copy-start(f32[256,2,1,160]{3,2,1,0:T(1,128)} %copy.654) | copy-start | bytes 983044
  257.3 16.9 %copy-start.16 = (f32[256,2,4,128]{3,2,1,0:T(4,128)S(1)}, f32[256,2,4,128]{3,2,1,0:T(4,128)}, u32[]{:S(2)}) copy-start(f32[256,2,4,128]{3,2,1,0:T(4,128)} %copy-done.14) | copy-start | bytes 3145732
  257.4 16.9 %copy-start.18 = (f32[256,2,4,128]{3,2,1,0:T(4,128)S(1)}, f32[256,2,4,128]{3,2,1,0:T(4,128)}, u32[]{:S(2)}) copy-start(f32[256,2,4,128]{3,2,1,0:T(4,128)} %copy-done.17) | copy-start | bytes 3145732
  257.4 16.9 %copy-start.20 = (f32[256,4,2,128]{3,2,1,0:T(2,128)S(1)}, f32[256,4,2,128]{3,2,1,0:T(2,128)}, u32[]{:S(2)}) copy-start(f32[256,4,2,128]{3,2,1,0:T(2,128)} %copy-done.19) | copy-start | bytes 3145732
  257.4 16.9 %copy-start.25 = (f32[256,2,8,8]{3,2,1,0:T(8,128)S(1)}, f32[256,2,8,8]{3,2,1,0:T(8,128)}, u32[]{:S(2)}) copy-start(f32[256,2,8,8]{3,2,1,0:T(8,128)} %broadcast_subtract_fusion) | copy-start | bytes 393220
  257.4 16.9 %copy-start.35 = (f32[256,4,8]{2,1,0:T(4,128)S(1)}, f32[256,4,8]{2,1,0:T(4,128)}, u32[]{:S(2)}) copy-start(f32[256,4,8]{2,1,0:T(4,128)} %copy.617) | copy-start | bytes 98308
  257.4 16.9 %copy-start.40 = (f32[256,2,4]{2,1,0:T(2,128)S(1)}, f32[256,2,4]{2,1,0:T(2,128)}, u32[]{:S(2)}) copy-start(f32[256,2,4]{2,1,0:T(2,128)} %copy-done.39) | copy-start | bytes 24580
  278.6 4.6 copy-start.24
  283.2 9.6 %copy-start.38 = (bf16[2,32,2048]{2,1,0:T(8,128)(2,1)S(1)}, bf16[2,32,2048]{2,1,0:T(8,128)(2,1)}, u32[]{:S(2)}) copy-start(bf16[2,32,2048]{2,1,0:T(8,128)(2,1)} %param.31) | copy-start | bytes 786436
  297.2 1.1 copy-start.32
  475.8 6.3 %copy-start.1 = (bf16[2048,256]{1,0:T(8,128)(2,1)S(1)}, bf16[2048,256]{1,0:T(8,128)(2,1)}, u32[]{:S(2)}) copy-start(bf16[2048,256]{1,0:T(8,128)(2,1)} %param.23) | copy-start | bytes 3145732
  (4 other events, 3.5 us)
Sparse Core Ops, SparseCore 0:
  10.9 65.0 all-gather.1
  297.4 178.3 all-reduce.3
where the time goes:
time: 496 us; the launch traced here: 489 us
  waiting for transfers between devices  218 us (44%)
  matrix products  108 us (22%)
  local copies, waits for them, and re-layouts  89.5 us (18%)
  other arithmetic  52.6 us (11%)
  between operations  15.5 us (3%)
  blocking collectives  6.36 us (1%)
    psum x1, waiting for transfers between devices, on_device(): totals = lax.psum(partial_out, ('kv', 'tp'))  159 us
    dot_general x10, matrix products, exact_product(): return jnp.einsum(form, left, right, precision=lax.Precision.HIGHEST)  90 us
    all_gather x1, waiting for transfers between devices, on_device(): gathered = lax.all_gather(tokens, ('kv', 'tp'), axis=2, tiled=True)  58.3 us
    another operation x8, local copies, waits for them, and re-layouts, delta_recursion(): solution = jnp.stack(solved, axis=2)  22.3 us
    another operation x2, local copies, waits for them, and re-layouts, delta_recursion(): jnp.stack(solved, axis=2)  12.1 us
    unnamed x110, local copies, waits for them, and re-layouts  11 us
    concatenate x1, other arithmetic, delta_recursion(): jnp.concatenate([beta_all[..., None] * values_all, (beta_all * jnp.exp(ga...  10.5 us
  transfers between devices with their start and end apart: 2, of which 2 were waited for; matrix products, arithmetic and copies ran while one was open for 6% of the time, Pallas kernels for 0%

commit v1 on v0

--- a/solution.py
+++ b/solution.py
@@ -215,7 +215,9 @@
         blended_rows, output_weight.reshape(-1, width), preferred_element_type=jnp.float32
     )
     own_cols = output_norm_gain.shape[0]
-    totals = lax.psum(partial_out, ("kv", "tp"))
+    totals = partial_out
+    for src_i in ("tp", "kv"):
+        totals = lax.psum(totals, src_i)
     scaling = lax.rsqrt(jnp.mean(totals * totals, axis=-1, keepdims=True) + epsilon)
     own_index = lax.axis_index("kv") * lax.axis_size("tp") + lax.axis_index("tp")
     share = lax.dynamic_slice_in_dim(totals, own_index * own_cols, own_cols, 1)

time: 496 us -> 744 us (1.50)
  waiting for transfers between devices: 218 us -> 465 us
    psum x1 -> x2, waiting for transfers between devices: 159 us -> 406 us  [on_device(): totals = lax.psum(totals, src_i)]
  transfers between devices with their start and end apart: 2 -> 3, of which waited for: 2 -> 3; matrix products, arithmetic and copies ran while one was open for 6% -> 4% of each run, Pallas kernels for 0% -> 0%
where the time goes in v1:
time: 744 us; the launch traced here: 737 us
  waiting for transfers between devices  465 us (62%)
  matrix products  108 us (15%)
  local copies, waits for them, and re-layouts  89.2 us (12%)
  other arithmetic  52.6 us (7%)
  between operations  15.2 us (2%)
    psum x2, waiting for transfers between devices, on_device(): totals = lax.psum(totals, src_i)  406 us
    dot_general x10, matrix products, exact_product(): return jnp.einsum(form, left, right, precision=lax.Precision.HIGHEST)  90.3 us
    all_gather x1, waiting for transfers between devices, on_device(): gathered = lax.all_gather(tokens, ('kv', 'tp'), axis=2, tiled=True)  58.3 us
    another operation x8, local copies, waits for them, and re-layouts, delta_recursion(): solution = jnp.stack(solved, axis=2)  22.3 us
  transfers between devices with their start and end apart: 3, of which 3 were waited for; matrix products, arithmetic and copies ran while one was open for 4% of the time, Pallas kernels for 0%

profile of v1, /device:TPU:0, one launch (start us, length us, event | category | flops | bytes accessed | tf_op | source)
XLA Modules:
  0.0 736.9 jit_solution(17001707705488860015)
XLA Ops:
  11.4 2.1 fusion.18
  16.0 1.6 fusion.16
  17.7 58.3 %all-gather.2.cloned.1.call-done = bf16[256,4,2048]{0,2,1:T(8,128)(2,1)} async-done(((bf16[256,4,64]{0,2,1:T(8,128)(2,1)}), bf16[256,4,2048]{0,2,1:T(8,128)(2,1)}) %all-gather.2.cloned.1.call-update) | async-done | bytes 4194320 | tf_op jit(solution)/shard_map/all_gather | solution.py:174
  76.1 3.2 fusion
  79.5 2.7 fusion.2
  82.2 7.9 %copy.594 = bf16[256,4,2048]{2,1,0:T(4,128)(2,1)} copy(bf16[256,4,2048]{0,2,1:T(8,128)(2,1)} %fusion.2) | data formatting | bytes 8388608 | tf_op jit(solution)/shard_map/convert_element_type | solution.py:179
  90.2 3.0 fusion.61
  94.6 2.5 fusion.94
  98.4 6.9 reshape.134
  105.2 3.4 fusion.9
  111.1 1.7 bitcast_multiply_fusion
  112.8 1.7 broadcast_subtract_fusion
  115.3 5.3 multiply_multiply_fusion
  126.6 1.4 copy.663
  128.1 3.4 fusion.10
  133.5 15.6 %fusion.22 = f32[256,2,4,32]{3,2,1,0:T(4,128)S(1)} fusion(f32[256,2,32,128]{3,2,1,0:T(8,128)} %param.33, f32[256,4,2,128]{3,2,1,0:T(2,128)S(1)} %reshape.152, f32[256,2,4]{2,1,0:T(2,128)S(1)} %copy.609, f32[256,2,4]{2,1,0:T(2,128)S(1)} %copy.597), kind=kOutput, calls=%fused_computation.58 | convolution fusion | flops 101187584 | bytes 9715712 | tf_op jit(solution)/shard_map/bhid,bhed->bhie/dot_general | solution.py:14
  150.5 1.9 fusion.8
  155.5 1.7 convert_multiply_fusion.2
  157.2 10.5 %pad_maximum_fusion.7 = (f32[256,2,1,160]{3,2,1,0:T(1,128)}, f32[256,2,1,160]{3,2,1,0:T(1,128)S(1)}, f32[256,2,1,160]{3,2,1,0:T(1,128)S(1)}, f32[256,2,1,160]{3,...) fusion(f32[256,2,8,128]{3,2,1,0:T(8,128)S(1)} %fusion.8, ...), kind=kLoop, calls=%fused_computation.72 | loop fusion | flops 655360 | bytes 5242880 | tf_op jit(solution)/shard_map/concatenate | solution.py:109
  170.8 7.6 %fusion.24 = f32[256,2,1,160]{3,2,1,0:T(1,128)} fusion(f32[256,2,1,160]{3,2,1,0:T(1,128)S(1)} %copy.650, f32[256,2,1,160]{3,2,1,0:T(1,128)S(1)} %get-tuple-element.41, f32[256,2,8,8]{3,2,1,0:T(8,128)} %copy-done.6), kind=kOutput, calls=%fused_computation.60 | convolution fusion | flops 2129920 | bytes 1245184 | tf_op jit(solution)/shard_map/bhj,bhjd->bhd/dot_general | solution.py:14
  182.9 2.0 copy.633
  184.9 1.9 constant_dynamic-update-slice_fusion.7
  186.8 2.1 copy.652
  188.9 8.4 %fusion.5 = f32[256,2,1,160]{3,2,1,0:T(1,128)} fusion(f32[256,2,1,160]{3,2,1,0:T(1,128)} %copy.652, f32[256,2,1,160]{3,2,1,0:T(1,128)} %copy.651, f32[256,2,1,160]{3,2,1,0:T(1,128)} %copy-done.8, f32[256,2,1,160]{3,2,1,0:T(1,128)S(1)} %get-tuple-element.41, f32[256,2,8,8]{3,2,1,0:T(8,128)S(1)} %copy-done.7), kind=kOutput, calls=%fused_computation.28 | convolution fusion | flops 4915200 | bytes 2097152 | tf_op jit(solution)/shard_map/bhj,bhjd->bhd/dot_general | solution.py:14
  197.3 1.8 copy.686
  199.1 1.8 copy.635
  201.0 1.9 constant_dynamic-update-slice_fusion.6
  202.9 1.9 copy.653
  206.4 1.7 constant_dynamic-update-slice_fusion.1
  210.3 1.6 multiply_reduce_fusion.2
  212.9 1.9 copy.654
  216.3 1.8 multiply_reduce_fusion.1
  218.9 1.9 copy.655
  220.7 11.4 %stack.101 = f32[256,2,7,160]{3,2,1,0:T(8,128)} concatenate(f32[256,2,1,160]{3,2,1,0:T(1,128)S(1)} %get-tuple-element.41, f32[256,2,1,160]{3,2,1,0:T(1,128)S(1)} %copy-done.9, f32[256,2,1,160]{3,2,1,0:T(1,128)} %copy.651, f32[256,2,1,160]{3,2,1,0:T(1,128)} %copy.652, f32[256,2,1,160]{3,2,1,0:T(1,128)} %copy.653, f32[256,2,1,160]{3,2,1,0:T(1,128)} %copy.654, f32[256,2,1,160]{3,2,1,0:T(1,128)} %copy.655), dimensions={2} | concatenate | bytes 4587520 | tf_op jit(solution)/shard_map/stack | solution.py:118
  232.2 7.2 fusion.48
  240.7 1.9 copy.643
  242.5 1.7 fusion.40
  244.3 1.9 copy.656
  246.2 11.2 %stack.103 = f32[256,2,8,160]{3,2,1,0:T(8,128)} concatenate(f32[256,2,1,160]{3,2,1,0:T(1,128)S(1)} %get-tuple-element.41, f32[256,2,1,160]{3,2,1,0:T(1,128)S(1)} %copy-done.9, f32[256,2,1,160]{3,2,1,0:T(1,128)S(1)} %copy-done.10, f32[256,2,1,160]{3,2,1,0:T(1,128)S(1)} %copy-done.11, f32[256,2,1,160]{3,2,1,0:T(1,128)S(1)} %copy-done.12, f32[256,2,1,160]{3,2,1,0:T(1,128)S(1)} %copy-done.13, ...), dimensions={2} | concatenate | bytes 5242880 | tf_op jit(solution)/shard_map/stack | solution.py:121
  257.4 16.8 %slice_subtract_fusion = f32[256,2,8,32]{3,2,1,0:T(8,128)S(1)} fusion(f32[256,2,8,160]{3,2,1,0:T(8,128)} %stack.103, f32[256,2,32,128]{3,2,1,0:T(8,128)} %param.33), kind=kOutput, calls=%fused_computation.23 | convolution fusion | flops 201457664 | bytes 11534336 | tf_op jit(solution)/shard_map/bhcd,bhed->bhce/dot_general | solution.py:14
  274.3 4.2 convolution_multiply_fusion
  278.6 3.4 fusion.95
  284.3 6.4 psum.21
  292.5 4.6 fusion.96
  297.2 152.4 %all-reduce.5.cloned.1.call-done = f32[1024,2048]{1,0:T(8,128)} async-done(((f32[1024,2048]{1,0:T(8,128)}), f32[1024,2048]{1,0:T(8,128)}) %all-reduce.5.cloned.1.call-update) | async-done | bytes 8388624 | tf_op jit(solution)/shard_map/psum | solution.py:220
  450.7 19.1 %multiply_add_fusion = f32[256,2,32,128]{3,2,1,0:T(8,128)} fusion(f32[256,2,32,128]{3,2,1,0:T(8,128)} %param.33, f32[256,2]{1,0:T(8,128)S(1)} %bitcast.222, f32[256,2,8,32]{3,2,1,0:T(8,128)S(1)} %slice_subtract_fusion, f32[256,2,4]{2,1,0:T(2,128)S(1)} %copy.666, bf16[256,4,256]{2,1,0:T(4,128)(2,1)S(1)} %copy-done.26, f32[256,2,4]{2,1,0:T(2,128)S(1)} %copy-done.32), kind=kOutput, calls=%fused_computation.19 | convolution fusion | flops 105644032 | bytes 19005440 | tf_op jit(solution)/shard_map/bhcd,bhce->bhed/dot_general | solution.py:14
  469.8 253.8 %all-reduce.7.cloned.1.call-done = f32[1024,2048]{1,0:T(8,128)} async-done(((f32[1024,2048]{1,0:T(8,128)}), f32[1024,2048]{1,0:T(8,128)}) %all-reduce.7.cloned.1.call-update) | async-done | bytes 8388624 | tf_op jit(solution)/shard_map/psum | solution.py:220
  723.6 4.1 multiply_reduce_fusion
  (205 shorter events, 48.2 us)
Async XLA Ops:
  7.2 98.1 %copy-start = (bf16[2048,256]{1,0:T(8,128)(2,1)S(1)}, bf16[2048,256]{1,0:T(8,128)(2,1)}, u32[]{:S(2)}) copy-start(bf16[2048,256]{1,0:T(8,128)(2,1)} %param.23) | copy-start | bytes 3145732
  7.2 7.7 %copy-start.41 = (bf16[256,4,2,32]{0,3,2,1:T(8,128)(2,1)S(1)}, bf16[256,4,2,32]{0,3,2,1:T(8,128)(2,1)}, u32[]{:S(2)}) copy-start(bf16[256,4,2,32]{0,3,2,1:T(8,128)(2,1)} %param.35) | copy-start | bytes 393220
  7.2 8.8 %copy-start.47 = (s32[256]{0:T(256)S(1)}, s32[256]{0:T(256)}, u32[]{:S(2)}) copy-start(s32[256]{0:T(256)} %param.38) | copy-start | bytes 3076
  7.2 8.8 %copy-start.44 = (f32[256,4,2]{0,2,1:T(2,128)S(1)}, f32[256,4,2]{0,2,1:T(2,128)}, u32[]{:S(2)}) copy-start(f32[256,4,2]{0,2,1:T(2,128)} %param.36) | copy-start | bytes 24580
  7.2 8.8 %copy-start.45 = (f32[256,4,2]{0,2,1:T(2,128)S(1)}, f32[256,4,2]{0,2,1:T(2,128)}, u32[]{:S(2)}) copy-start(f32[256,4,2]{0,2,1:T(2,128)} %param.37) | copy-start | bytes 24580
  7.2 68.8 %all-gather.2.cloned.1.call-start = ((), (), s32[]{:S(2)}) async-start(), calls=%async_computation | async-start | bytes 4325376 | tf_op jit(solution)/shard_map/all_gather | solution.py:174
  8.0 441.6 %all-reduce.5.cloned.1.call-start = ((), (), s32[]{:S(2)}) async-start(), calls=%async_computation.1 | async-start | bytes 16777216 | tf_op jit(solution)/shard_map/psum | solution.py:220
  11.4 83.1 %copy-start.21 = (f32[256,8,8]{2,1,0:T(8,128)}, f32[256,8,8]{2,1,0:T(8,128)S(1)}, u32[]{:S(2)}) copy-start(f32[256,8,8]{2,1,0:T(8,128)S(1)} %copy.607) | copy-start | bytes 196612
  13.9 65.3 %copy-start.31 = (f32[256,2,4]{2,1,0:T(2,128)}, f32[256,2,4]{2,1,0:T(2,128)S(1)}, u32[]{:S(2)}) copy-start(f32[256,2,4]{2,1,0:T(2,128)S(1)} %copy.611) | copy-start | bytes 24580
  17.7 97.6 %copy-start.14 = (f32[256,2,4,128]{3,2,1,0:T(4,128)}, f32[256,2,4,128]{3,2,1,0:T(4,128)S(1)}, u32[]{:S(2)}) copy-start(f32[256,2,4,128]{3,2,1,0:T(4,128)S(1)} %fusion.16) | copy-start | bytes 3145732
  76.1 3.4 copy-start.5
  82.2 7.9 %copy-start.42 = (bf16[2048,2]{0,1:T(2,128)(2,1)S(1)}, bf16[2048,2]{0,1:T(2,128)(2,1)}, u32[]{:S(2)}) copy-start(bf16[2048,2]{0,1:T(2,128)(2,1)} %param.27) | copy-start | bytes 24580
  90.2 3.4 copy-start.2
  90.2 3.5 copy-start.43
  112.8 7.9 %copy-start.17 = (f32[256,2,4,128]{3,2,1,0:T(4,128)}, f32[256,2,4,128]{3,2,1,0:T(4,128)S(1)}, u32[]{:S(2)}) copy-start(f32[256,2,4,128]{3,2,1,0:T(4,128)S(1)} %bitcast_multiply_fusion) | copy-start | bytes 3145732
  112.8 2.5 copy-start.22
  115.3 9.1 %copy-start.3 = (bf16[1024,2048]{1,0:T(8,128)(2,1)S(1)}, bf16[1024,2048]{1,0:T(8,128)(2,1)}, u32[]{:S(2)}) copy-start(bf16[1024,2048]{1,0:T(8,128)(2,1)} %reshape.134) | copy-start | bytes 12582916
  120.7 2.8 copy-start.6
  120.7 3.7 copy-start.36
  125.8 2.3 copy-start.48
  132.1 1.4 copy-start.19
  133.5 15.6 %copy-start.39 = (f32[256,2,4]{2,1,0:T(2,128)}, f32[256,2,4]{2,1,0:T(2,128)S(1)}, u32[]{:S(2)}) copy-start(f32[256,2,4]{2,1,0:T(2,128)S(1)} %copy.597) | copy-start | bytes 24580
  149.1 1.4 copy-start.15
  150.5 2.5 copy-start.4
  150.5 2.5 copy-start.37
  157.2 11.8 %copy-start.34 = (f32[256,2,1,1]{3,2,1,0:T(1,128)S(1)}, f32[256,2,1,1]{3,2,1,0:T(1,128)}, u32[]{:S(2)}) copy-start(f32[256,2,1,1]{3,2,1,0:T(1,128)} %slice.141) | copy-start | bytes 6148
  170.8 7.6 %copy-start.8 = (f32[256,2,1,160]{3,2,1,0:T(1,128)}, f32[256,2,1,160]{3,2,1,0:T(1,128)S(1)}, u32[]{:S(2)}) copy-start(f32[256,2,1,160]{3,2,1,0:T(1,128)S(1)} %copy.650) | copy-start | bytes 983044
  170.8 8.9 %copy-start.29 = (f32[256,2,1,160]{3,2,1,0:T(1,128)S(1)}, f32[256,2,1,160]{3,2,1,0:T(1,128)}, u32[]{:S(2)}) copy-start(f32[256,2,1,160]{3,2,1,0:T(1,128)} %get-tuple-element.43) | copy-start | bytes 983044
  178.4 3.5 copy-start.33
  182.9 6.0 copy-start.7
  204.8 3.2 copy-start.23
  205.6 4.3 copy-start.28
  210.3 5.5 copy-start.27
  216.3 4.5 copy-start.9
  239.3 6.8 copy-start.10
  239.3 6.9 copy-start.11
  239.3 6.9 copy-start.12
  239.3 6.9 copy-start.13
  257.3 16.9 %copy-start.16 = (f32[256,2,4,128]{3,2,1,0:T(4,128)S(1)}, f32[256,2,4,128]{3,2,1,0:T(4,128)}, u32[]{:S(2)}) copy-start(f32[256,2,4,128]{3,2,1,0:T(4,128)} %copy-done.14) | copy-start | bytes 3145732
  257.4 16.9 %copy-start.18 = (f32[256,2,4,128]{3,2,1,0:T(4,128)S(1)}, f32[256,2,4,128]{3,2,1,0:T(4,128)}, u32[]{:S(2)}) copy-start(f32[256,2,4,128]{3,2,1,0:T(4,128)} %copy-done.17) | copy-start | bytes 3145732
  257.4 16.9 %copy-start.20 = (f32[256,4,2,128]{3,2,1,0:T(2,128)S(1)}, f32[256,4,2,128]{3,2,1,0:T(2,128)}, u32[]{:S(2)}) copy-start(f32[256,4,2,128]{3,2,1,0:T(2,128)} %copy-done.19) | copy-start | bytes 3145732
  257.4 16.9 %copy-start.25 = (f32[256,2,8,8]{3,2,1,0:T(8,128)S(1)}, f32[256,2,8,8]{3,2,1,0:T(8,128)}, u32[]{:S(2)}) copy-start(f32[256,2,8,8]{3,2,1,0:T(8,128)} %broadcast_subtract_fusion) | copy-start | bytes 393220
  257.4 16.9 %copy-start.35 = (f32[256,4,8]{2,1,0:T(4,128)S(1)}, f32[256,4,8]{2,1,0:T(4,128)}, u32[]{:S(2)}) copy-start(f32[256,4,8]{2,1,0:T(4,128)} %copy.617) | copy-start | bytes 98308
  257.4 16.9 %copy-start.40 = (f32[256,2,4]{2,1,0:T(2,128)S(1)}, f32[256,2,4]{2,1,0:T(2,128)}, u32[]{:S(2)}) copy-start(f32[256,2,4]{2,1,0:T(2,128)} %copy-done.39) | copy-start | bytes 24580
  278.6 4.6 copy-start.24
  283.2 9.3 %copy-start.38 = (bf16[2,32,2048]{2,1,0:T(8,128)(2,1)S(1)}, bf16[2,32,2048]{2,1,0:T(8,128)(2,1)}, u32[]{:S(2)}) copy-start(bf16[2,32,2048]{2,1,0:T(8,128)(2,1)} %param.31) | copy-start | bytes 786436
  297.1 426.5 %all-reduce.7.cloned.1.call-start = ((), (), s32[]{:S(2)}) async-start(), calls=%async_computation.2 | async-start | bytes 16777216 | tf_op jit(solution)/shard_map/psum | solution.py:220
  723.6 6.3 copy-start.1
  (5 other events, 4.6 us)
Sparse Core Ops, SparseCore 0:
  10.9 65.0 all-gather.1
  297.3 152.2 all-reduce.4
  453.4 270.1 all-reduce.6
